TPU v7x, 32 devices: a whole 2x2x4 slice. The times are simulated.
32 devices in a mesh: ep: 16 (over z, y, core), tp: 2 (over x).
Axes of the slice: x: 2, y: 2, z: 4, core: 2. Of those that a mesh axis runs over, the one named last changes fastest.
Arguments:
- tokens: bfloat16 [256, 2048], P('ep'), may hold values from -6 to 6
- recur_state: float32 [256, 8, 128, 128], P('ep', 'tp'), may hold values from -0.4 to 0.4
- attn_gain: float32 [2048], replicated, may hold values from 0.1 to 1.9
- query_weight: bfloat16 [2048, 1024], P(None, 'tp'), may hold values from -0.125 to 0.125
- key_weight: bfloat16 [2048, 1024], P(None, 'tp'), may hold values from -0.125 to 0.125
- value_weight: bfloat16 [2048, 1024], P(None, 'tp'), may hold values from -0.125 to 0.125
- outgate_weight: bfloat16 [2048, 1024], P(None, 'tp'), may hold values from -0.125 to 0.125
- beta_weight: bfloat16 [2048, 8], replicated, may hold values from -0.125 to 0.125
- decay_weight: bfloat16 [2048, 8], replicated, may hold values from -0.125 to 0.125
- decay_rate: float32 [8], replicated, may hold values from 0.05 to 2
- head_gain: float32 [128], replicated, may hold values from 0.1 to 1.9
- output_weight: bfloat16 [1024, 2048], P('tp'), may hold values from -0.1875 to 0.1875
- ffn_gain: float32 [2048], replicated, may hold values from 0.1 to 1.9
- routes: int32 [256, 2], P('ep'), may hold values from 0 to 3, all different within a row; in each aligned block of 16 rows (0 to 15, 16 to 31, ...) at most 16 rows name the same one
- route_weight: float32 [256, 2], P('ep'), may hold values from 0.2 to 1
- expert_gate: bfloat16 [16, 2048, 1024], P('ep', None, 'tp'), may hold values from -0.125 to 0.125
- expert_up: bfloat16 [16, 2048, 1024], P('ep', None, 'tp'), may hold values from -0.125 to 0.125
- expert_down: bfloat16 [16, 1024, 2048], P('ep', 'tp'), may hold values from -0.09375 to 0.09375
Outputs:
- mixed: bfloat16 [256, 2048], P('ep', 'tp')
- new_state: float32 [256, 8, 128, 128], P('ep', 'tp')
Inputs may be any that keep to these rules, and one draw needn't show every extreme that they name: `routes`: each row names 2 different experts; in each aligned block of 16 rows no expert is named by more than 16 rows.
All inputs are finite; a program needn't handle non-finite values.
Results may differ from a plain program's by a relative error of at most 0.014.
Values may be sent and summed in bfloat16 or wider, within the bound.
A program may use at most 64 MiB of HBM per device.

v0:
```python
import jax
import jax.numpy as jnp
from jax import lax
from jax.sharding import PartitionSpec as P

EPS = 1e-06


def rms_scale(values, gain):
    return values * lax.rsqrt(jnp.mean(values * values, axis=-1, keepdims=True) + EPS) * gain


def unit_rows(values):
    return values * lax.rsqrt(jnp.sum(values * values, axis=-1, keepdims=True) + EPS)


def slot_targets(group_routes, experts, capacity):
    flat = group_routes.reshape(-1)
    onehot = (flat[:, None] == jnp.arange(experts, dtype=jnp.int32)[None, :]).astype(jnp.int32)
    running = jnp.cumsum(onehot, axis=0)
    position = jnp.sum(running * onehot, axis=1) - 1
    return (flat * capacity + position).reshape(group_routes.shape)


def local(
    tokens,
    recur_state,
    attn_gain,
    query_weight,
    key_weight,
    value_weight,
    outgate_weight,
    beta_weight,
    decay_weight,
    decay_rate,
    head_gain,
    output_weight,
    ffn_gain,
    routes,
    route_weight,
    expert_gate,
    expert_up,
    expert_down,
):
    f32 = jnp.float32
    bf16 = jnp.bfloat16
    highest = lax.Precision.HIGHEST
    seq_count, model_width = tokens.shape
    heads_here = recur_state.shape[1]
    head_size = recur_state.shape[2]
    groups = lax.axis_size("ep")
    lanes = lax.axis_size("tp")
    lane_index = lax.axis_index("tp")
    normed = rms_scale(tokens.astype(f32), attn_gain).astype(bf16)
    qproj = jnp.dot(normed, query_weight, preferred_element_type=f32).astype(bf16)
    kproj = jnp.dot(normed, key_weight, preferred_element_type=f32).astype(bf16)
    vproj = jnp.dot(normed, value_weight, preferred_element_type=f32).astype(bf16)
    zproj = jnp.dot(normed, outgate_weight, preferred_element_type=f32).astype(bf16)
    first_head = lane_index * heads_here
    own_beta = lax.dynamic_slice_in_dim(beta_weight, first_head, heads_here, 1)
    own_decay = lax.dynamic_slice_in_dim(decay_weight, first_head, heads_here, 1)
    own_rate = lax.dynamic_slice_in_dim(decay_rate, first_head, heads_here, 0)
    strength = jax.nn.sigmoid(jnp.dot(normed, own_beta, preferred_element_type=f32))
    fading = jnp.exp(
        -own_rate * jax.nn.softplus(jnp.dot(normed, own_decay, preferred_element_type=f32))
    )

    def split_heads(proj):
        return proj.astype(f32).reshape(seq_count, heads_here, head_size)

    query = unit_rows(jax.nn.silu(split_heads(qproj))) * head_size ** (-0.5)
    keyvec = unit_rows(jax.nn.silu(split_heads(kproj)))
    value = jax.nn.silu(split_heads(vproj))
    recall = jnp.einsum("thd,thde->the", keyvec, recur_state, precision=highest)
    written = (strength[..., None] * keyvec)[..., :, None] * (value - fading[..., None] * recall)[
        ..., None, :
    ]
    new_state = fading[..., None, None] * recur_state + written
    readout = jnp.einsum("thd,thde->the", query, new_state, precision=highest)
    headed = (
        (rms_scale(readout, head_gain) * jax.nn.silu(split_heads(zproj)))
        .reshape(seq_count, heads_here * head_size)
        .astype(bf16)
    )
    partial_out = jnp.dot(headed, output_weight, preferred_element_type=f32)
    branch = lax.psum(partial_out, "tp").astype(bf16)
    resid = (tokens.astype(f32) + branch.astype(f32)).astype(bf16)
    ffn_in = rms_scale(resid.astype(f32), ffn_gain).astype(bf16)
    top_count = routes.shape[1]
    experts = groups // 4
    capacity = min(seq_count, max(2, (2 * seq_count * top_count + experts - 1) // experts))
    quarter = model_width // lanes
    targets = slot_targets(routes, experts, capacity)
    slot_ids = jnp.arange(experts * capacity, dtype=jnp.int32)
    select = jnp.any(slot_ids[:, None, None] == targets[None, :, :], axis=-1).astype(bf16)
    gate_local = expert_gate[0]
    up_local = expert_up[0]
    down_local = expert_down[0]
    packed = jnp.dot(select, ffn_in, preferred_element_type=f32).astype(bf16)
    packed = packed.reshape(experts, 1, capacity, ffn_in.shape[1])
    packed = jnp.broadcast_to(packed, (experts, 4, capacity, ffn_in.shape[1]))
    arrived = lax.all_to_all(
        packed.reshape(groups, capacity, ffn_in.shape[1]),
        "ep",
        split_axis=0,
        concat_axis=0,
        tiled=True,
    ).reshape(groups * capacity, model_width)
    gated = jnp.dot(arrived, gate_local, preferred_element_type=f32)
    lifted = jnp.dot(arrived, up_local, preferred_element_type=f32)
    hidden = (jax.nn.silu(gated) * lifted).astype(bf16)
    slice_terms = jnp.dot(hidden, down_local, preferred_element_type=f32).reshape(
        groups, capacity, model_width
    )
    shares = lax.psum_scatter(slice_terms, "tp", scatter_dimension=2, tiled=True).astype(bf16)
    returned = lax.all_to_all(shares, "ep", split_axis=0, concat_axis=0, tiled=True)
    merged = (
        returned.astype(f32)
        .reshape(experts, 4, capacity, quarter)
        .sum(axis=1)
        .reshape(experts * capacity, quarter)
    )
    combine = jnp.zeros((seq_count, experts * capacity), f32)
    for choice_idx in range(top_count):
        match = (targets[:, choice_idx, None] == slot_ids[None, :]).astype(f32)
        combine = combine + route_weight[:, choice_idx, None] * match
    moe = jnp.dot(combine, merged, precision=highest)
    resid_own = lax.dynamic_slice_in_dim(resid, lane_index * quarter, quarter, 1)
    mixed = (resid_own.astype(f32) + moe).astype(bf16)
    return (mixed, new_state)


def solution(mesh):
    return jax.shard_map(
        local,
        mesh=mesh,
        in_specs=(
            P("ep", None),
            P("ep", "tp", None, None),
            P(),
            P(None, "tp"),
            P(None, "tp"),
            P(None, "tp"),
            P(None, "tp"),
            P(),
            P(),
            P(),
            P(),
            P("tp", None),
            P(),
            P("ep", None),
            P("ep", None),
            P("ep", None, "tp"),
            P("ep", None, "tp"),
            P("ep", "tp", None),
        ),
        out_specs=(P("ep", "tp"), P("ep", "tp", None, None)),
        check_vma=False,
    )
```

profile of v0, /device:TPU:0, one launch (start us, length us, event | category | flops | bytes accessed | tf_op | source)
XLA Modules:
  0.0 138.9 jit_solution(11278963235603328612)
XLA Ops:
  7.3 1.1 fusion.23
  8.4 1.1 fusion.19
  9.5 2.1 %fusion.15 = f32[16,512]{1,0:T(8,128)S(1)} fusion(bf16[2048,512]{1,0:T(8,128)(2,1)} %param.22, bf16[16,2048]{1,0:T(8,128)(2,1)} %param.18, f32[2048]{0:T(1024)} %param.20, f32[16]{0:T(128)S(1)} %add_rsqrt_fusion.4), kind=kOutput, calls=%fused_computation.17 | convolution fusion | flops 33701888 | bytes 2203712 | tf_op jit(solution)/shard_map/dot_general | solution.py:56
  11.9 0.2 fusion.50
  12.2 2.0 %fusion.14 = f32[16,512]{1,0:T(8,128)S(1)} fusion(bf16[2048,512]{1,0:T(8,128)(2,1)} %param.23, bf16[16,2048]{1,0:T(8,128)(2,1)S(1)} %copy-done.3, f32[2048]{0:T(1024)S(1)} %copy-done.5, f32[16]{0:T(128)S(1)} %add_rsqrt_fusion.4), kind=kOutput, calls=%fused_computation.15 | convolution fusion | flops 33701888 | bytes 2203712 | tf_op jit(solution)/shard_map/dot_general | solution.py:57
  14.2 2.0 %fusion.16 = f32[16,512]{1,0:T(8,128)S(1)} fusion(bf16[2048,512]{1,0:T(8,128)(2,1)} %param.21, bf16[16,2048]{1,0:T(8,128)(2,1)S(1)} %copy-done.3, f32[2048]{0:T(1024)S(1)} %copy-done.5, f32[16]{0:T(128)S(1)} %add_rsqrt_fusion.4), kind=kOutput, calls=%fused_computation.19 | convolution fusion | flops 33701888 | bytes 2203712 | tf_op jit(solution)/shard_map/dot_general | solution.py:55
  16.6 5.5 %fusion.63 = f32[16,4,1,128]{3,2,1,0:T(1,128)S(1)} fusion(f32[16,4,128,1]{2,3,1,0:T(1,128)S(1)} %bitcast.66, f32[16,4,128,128]{3,2,1,0:T(8,128)} %param.19), kind=kOutput, calls=%fused_computation.91 | convolution fusion | flops 12582912 | bytes 4259840 | tf_op jit(solution)/shard_map/thd,thde->the/dot_general | solution.py:74
  22.2 1.5 %multiply_add_fusion = f32[16,4,128,128]{3,2,1,0:T(8,128)S(1)} fusion(f32[16,4,128,128]{3,2,1,0:T(8,128)S(1)} %copy-done.1, f32[16,4,128]{2,1,0:T(4,128)S(1)} %fusion.30, f32[16,4,128]{2,1,0:T(4,128)S(1)} %get-tuple-element.4, f32[16,4]{1,0:T(8,128)S(1)} %copy.39), kind=kLoop, calls=%fused_computation | loop fusion | flops 3145728 | bytes 8454400 | tf_op jit(solution)/shard_map/add | solution.py:78
  23.7 3.7 %fusion.64 = f32[16,4,1,128]{3,2,1,0:T(1,128)S(1)} fusion(f32[16,4,128,1]{2,3,1,0:T(1,128)S(1)} %bitcast.67, f32[16,4,128,128]{3,2,1,0:T(8,128)S(1)} %multiply_add_fusion), kind=kOutput, calls=%fused_computation.92 | convolution fusion | flops 12582912 | bytes 4259840 | tf_op jit(solution)/shard_map/thd,thde->the/dot_general | solution.py:79
  27.5 0.4 fusion.13
  28.1 2.0 %fusion.33 = f32[16,2048]{1,0:T(8,128)S(1)} fusion(bf16[512,2048]{1,0:T(8,128)(2,1)} %param.29, bf16[2,8,4,128]{3,2,1,0:T(4,128)(2,1)S(1)} %bitcast.69), kind=kOutput, calls=%fused_computation.50 | convolution fusion | flops 33554432 | bytes 2244608 | tf_op jit(solution)/shard_map/dot_general | solution.py:85
  30.1 11.3 %all-reduce.1 = bf16[16,2048]{1,0:T(8,128)(2,1)S(1)} all-reduce(f32[16,2048]{1,0:T(8,128)S(1)} %fusion.33), channel_id=1, replica_groups=mesh['ep'=16,'tp'=2] {'tp'}, use_global_device_ids=true, to_apply=%region_4.5 | all-reduce | flops 32768 | bytes 196608 | tf_op jit(solution)/shard_map/psum | solution.py:86
  41.9 0.2 select_reduce_fusion
  42.4 0.3 convolution_convert_fusion
  42.8 30.4 %all_to_all.10 = bf16[16,16,2048]{2,1,0:T(8,128)(2,1)S(1)} all-to-all(bf16[16,16,2048]{2,1,0:T(8,128)(2,1)S(1)} %bitcast.58), channel_id=1, replica_groups=mesh['ep'=16,'tp'=2] {'ep'}, dimensions={0} | all-to-all | bytes 2097152 | tf_op jit(solution)/shard_map/all_to_all | solution.py:102
  73.2 0.7 fusion.4
  73.9 0.9 copy-done.11
  74.7 0.7 fusion.9
  75.5 2.1 %fusion = f32[16,16,2048]{2,1,0:T(8,128)} fusion(bf16[16,16,512]{2,1,0:T(8,128)(2,1)S(1)} %bitcast.65, bf16[1,512,2048]{2,1,0:T(8,128)(2,1)S(1)} %copy-done), kind=kOutput, calls=%fused_computation.2 | convolution fusion | flops 536870912 | bytes 4456448 | tf_op jit(solution)/shard_map/dot_general | solution.py:112
  77.6 31.5 %reduce-scatter.2.cloned.1.call-done = f32[16,16,1024]{2,1,0:T(8,128)} async-done(((f32[16,16,2048]{2,1,0:T(8,128)}), f32[16,16,1024]{2,1,0:T(8,128)}) %reduce-scatter.2.cloned.1.call-update) | async-done | bytes 1048592 | tf_op jit(solution)/shard_map/reduce_scatter | solution.py:115
  109.1 2.1 %convert_element_type.83 = bf16[16,16,1024]{2,1,0:T(8,128)(2,1)} convert(f32[16,16,1024]{2,1,0:T(8,128)} %reduce-scatter.2.cloned.1.call-done) | non-fusion elementwise | flops 262144 | bytes 1572864 | tf_op jit(solution)/shard_map/convert_element_type | solution.py:115
  111.2 5.6 %all-to-all-start.1 = ((bf16[16,16,1024]{2,1,0:T(8,128)(2,1)}), bf16[16,16,1024]{2,1,0:T(8,128)(2,1)S(1)}, u32[]{:S(2)}, u32[]{:S(2)}) async-start(bf16[16,16,1024]{2,1,0:T(8,128)(2,1)} %convert_element_type.83), calls=%async_computation.2 | async-start | bytes 1048576 | tf_op jit(solution)/shard_map/all_to_all | solution.py:116
  116.8 14.2 %all-to-all-done.1 = bf16[16,16,1024]{2,1,0:T(8,128)(2,1)S(1)} async-done(((bf16[16,16,1024]{2,1,0:T(8,128)(2,1)}), bf16[16,16,1024]{2,1,0:T(8,128)(2,1)S(1)}, u32[]{:S(2)}, u32[]{:S(2)}) %all-to-all-start.1) | async-done | bytes 524320 | tf_op jit(solution)/shard_map/all_to_all | solution.py:116
  131.1 0.9 fusion.12
  (62 shorter events, 2.1 us)
Async XLA Ops:
  7.2 68.3 %copy-start = (bf16[1,512,2048]{2,1,0:T(8,128)(2,1)S(1)}, bf16[1,512,2048]{2,1,0:T(8,128)(2,1)}, u32[]{:S(2)}) copy-start(bf16[1,512,2048]{2,1,0:T(8,128)(2,1)} %param.35) | copy-start | bytes 6291460
  7.2 4.7 %copy-start.3 = (bf16[16,2048]{1,0:T(8,128)(2,1)S(1)}, bf16[16,2048]{1,0:T(8,128)(2,1)}, u32[]{:S(2)}) copy-start(bf16[16,2048]{1,0:T(8,128)(2,1)} %param.18) | copy-start | bytes 196612
  7.2 4.7 %copy-start.5 = (f32[2048]{0:T(1024)S(1)}, f32[2048]{0:T(1024)}, u32[]{:S(2)}) copy-start(f32[2048]{0:T(1024)} %param.20) | copy-start | bytes 24580
  7.2 4.6 %copy-start.13 = (f32[8]{0:T(128)S(1)}, f32[8]{0:T(128)}, u32[]{:S(2)}) copy-start(f32[8]{0:T(128)} %param.27) | copy-start | bytes 100
  7.2 4.7 %copy-start.12 = (bf16[2048,8]{0,1:T(8,128)(2,1)S(1)}, bf16[2048,8]{0,1:T(8,128)(2,1)}, u32[]{:S(2)}) copy-start(bf16[2048,8]{0,1:T(8,128)(2,1)} %param.26) | copy-start | bytes 98308
  7.2 101.8 %reduce-scatter.2.cloned.1.call-start = ((), (), s32[]{:S(2)}) async-start(), calls=%async_computation.3 | async-start | bytes 3145728 | tf_op jit(solution)/shard_map/reduce_scatter | solution.py:115
  16.6 5.6 %copy-start.1 = (f32[16,4,128,128]{3,2,1,0:T(8,128)S(1)}, f32[16,4,128,128]{3,2,1,0:T(8,128)}, u32[]{:S(2)}) copy-start(f32[16,4,128,128]{3,2,1,0:T(8,128)} %param.19) | copy-start | bytes 12582916
  23.7 3.7 %copy-start.2 = (f32[16,4,128,128]{3,2,1,0:T(8,128)}, f32[16,4,128,128]{3,2,1,0:T(8,128)S(1)}, u32[]{:S(2)}) copy-start(f32[16,4,128,128]{3,2,1,0:T(8,128)S(1)} %multiply_add_fusion) | copy-start | bytes 12582916
  23.7 3.8 %copy-start.4 = (bf16[2048,512]{1,0:T(8,128)(2,1)S(1)}, bf16[2048,512]{1,0:T(8,128)(2,1)}, u32[]{:S(2)}) copy-start(bf16[2048,512]{1,0:T(8,128)(2,1)} %param.24) | copy-start | bytes 6291460
  27.4 0.7 copy-start.9
  27.5 14.1 %copy-start.7 = (s32[16,2]{0,1:T(2,128)S(1)}, s32[16,2]{0,1:T(2,128)}, u32[]{:S(2)}) copy-start(s32[16,2]{0,1:T(2,128)} %param.31) | copy-start | bytes 388
  27.5 14.9 %copy-start.6 = (f32[2048]{0:T(1024)S(1)}, f32[2048]{0:T(1024)}, u32[]{:S(2)}) copy-start(f32[2048]{0:T(1024)} %param.30) | copy-start | bytes 24580
  42.3 30.9 %copy-start.10 = (bf16[1,2048,512]{2,1,0:T(8,128)(2,1)S(1)}, bf16[1,2048,512]{2,1,0:T(8,128)(2,1)}, u32[]{:S(2)}) copy-start(bf16[1,2048,512]{2,1,0:T(8,128)(2,1)} %param.33) | copy-start | bytes 6291460
  73.2 1.6 %copy-start.11 = (bf16[1,2048,512]{2,1,0:T(8,128)(2,1)S(1)}, bf16[1,2048,512]{2,1,0:T(8,128)(2,1)}, u32[]{:S(2)}) copy-start(bf16[1,2048,512]{2,1,0:T(8,128)(2,1)} %param.34) | copy-start | bytes 6291460
  77.5 39.3 %copy-start.8 = (f32[16,2]{0,1:T(2,128)S(1)}, f32[16,2]{0,1:T(2,128)}, u32[]{:S(2)}) copy-start(f32[16,2]{0,1:T(2,128)} %param.32) | copy-start | bytes 388
  111.2 19.9 %all-to-all-start.1 = ((bf16[16,16,1024]{2,1,0:T(8,128)(2,1)}), bf16[16,16,1024]{2,1,0:T(8,128)(2,1)S(1)}, u32[]{:S(2)}, u32[]{:S(2)}) async-start(bf16[16,16,1024]{2,1,0:T(8,128)(2,1)} %convert_element_type.83), calls=%async_computation.2 | async-start | bytes 1048576 | tf_op jit(solution)/shard_map/all_to_all | solution.py:116
Sparse Core Ops, SparseCore 0:
  77.7 31.3 reduce-scatter.1
where the time goes:
time: 139 us
  waiting for transfers between devices  45.8 us (33%)
  blocking collectives  41.7 us (30%)
  matrix products  23.6 us (17%)
  between operations  14.3 us (10%)
  other arithmetic  6.09 us (4%)
  starting transfers between devices  5.65 us (4%)
  local copies, waits for them, and re-layouts  1.71 us (1%)
    reduce_scatter x1, waiting for transfers between devices, local(): lax.psum_scatter(slice_terms, 'tp', scatter_dimension=2, tiled=True)  31.5 us
    all_to_all x1, blocking collectives, local(): lax.all_to_all(packed.reshape(groups, capacity, ffn_in.shape[1]), 'ep', s...  30.4 us
    all_to_all x1, waiting for transfers between devices, local(): lax.all_to_all(shares, 'ep', split_axis=0, concat_axis=0, tiled=True)  14.2 us
    psum x1, blocking collectives, local(): branch = lax.psum(partial_out, 'tp').astype(bf16)  11.3 us
    all_to_all x1, starting transfers between devices, local(): lax.all_to_all(shares, 'ep', split_axis=0, concat_axis=0, tiled=True)  5.61 us
    dot_general x1, matrix products, local(): recall = jnp.einsum('thd,thde->the', keyvec, recur_state, precision=highest)  5.48 us
    dot_general x1, matrix products, local(): readout = jnp.einsum('thd,thde->the', query, new_state, precision=highest)  3.66 us
  transfers between devices with their start and end apart: 2, of which 2 were waited for; matrix products, arithmetic and copies ran while one was open for 0% of the time, Pallas kernels for 0%

commit v1 on v0

--- a/solution.py
+++ b/solution.py
@@ -1,9 +1,17 @@
+import functools
 import jax
 import jax.numpy as jnp
 from jax import lax
 from jax.sharding import PartitionSpec as P
 
 EPS = 1e-06
+
+
+def unite_the_leaf(field_in, a_name):
+    return jnp.sum(lax.all_gather(field_in, a_name), axis=0)
+
+
+pools_time = functools.partial(unite_the_leaf, a_name="tp")
 
 
 def rms_scale(values, gain):
@@ -83,7 +91,7 @@
         .astype(bf16)
     )
     partial_out = jnp.dot(headed, output_weight, preferred_element_type=f32)
-    branch = lax.psum(partial_out, "tp").astype(bf16)
+    branch = pools_time(partial_out).astype(bf16)
     resid = (tokens.astype(f32) + branch.astype(f32)).astype(bf16)
     ffn_in = rms_scale(resid.astype(f32), ffn_gain).astype(bf16)
     top_count = routes.shape[1]

time: 139 us -> 137 us (0.986)
  blocking collectives: 41.7 us -> 37.9 us
    psum x1 -> x0, blocking collectives: 11.3 us -> none  [local(): branch = lax.psum(partial_out, 'tp').astype(bf16)]
    all_gather x0 -> x1, blocking collectives: none -> 7.11 us  [unite_the_leaf(): return jnp.sum(lax.all_gather(field_in, a_name), axis=0)]
where the time goes in v1:
time: 137 us; the launch traced here: 136 us
  waiting for transfers between devices  46.7 us (34%)
  blocking collectives  37.9 us (28%)
  matrix products  23.6 us (17%)
  between operations  14.3 us (10%)
  other arithmetic  6.11 us (4%)
  starting transfers between devices  5.65 us (4%)
  local copies, waits for them, and re-layouts  1.73 us (1%)
    reduce_scatter x1, waiting for transfers between devices, local(): lax.psum_scatter(slice_terms, 'tp', scatter_dimension=2, tiled=True)  32.4 us
    all_to_all x1, blocking collectives, local(): lax.all_to_all(packed.reshape(groups, capacity, ffn_in.shape[1]), 'ep', s...  30.8 us
    all_to_all x1, waiting for transfers between devices, local(): lax.all_to_all(shares, 'ep', split_axis=0, concat_axis=0, tiled=True)  14.2 us
    all_gather x1, blocking collectives, unite_the_leaf(): return jnp.sum(lax.all_gather(field_in, a_name), axis=0)  7.11 us
    all_to_all x1, starting transfers between devices, local(): lax.all_to_all(shares, 'ep', split_axis=0, concat_axis=0, tiled=True)  5.61 us
    dot_general x1, matrix products, local(): recall = jnp.einsum('thd,thde->the', keyvec, recur_state, precision=highest)  5.48 us
    dot_general x1, matrix products, local(): readout = jnp.einsum('thd,thde->the', query, new_state, precision=highest)  3.66 us
  transfers between devices with their start and end apart: 2, of which 2 were waited for; matrix products, arithmetic and copies ran while one was open for 0% of the time, Pallas kernels for 0%

profile of v1, /device:TPU:0, one launch (start us, length us, event | category | flops | bytes accessed | tf_op | source)
XLA Modules:
  0.0 136.0 jit_solution(8932454595161598915)
XLA Ops:
  7.3 1.1 fusion.23
  8.4 1.1 fusion.19
  9.5 2.1 %fusion.15 = f32[16,512]{1,0:T(8,128)S(1)} fusion(bf16[2048,512]{1,0:T(8,128)(2,1)} %param.22, bf16[16,2048]{1,0:T(8,128)(2,1)} %param.18, f32[2048]{0:T(1024)} %param.20, f32[16]{0:T(128)S(1)} %add_rsqrt_fusion.4), kind=kOutput, calls=%fused_computation.17 | convolution fusion | flops 33701888 | bytes 2203712 | tf_op jit(solution)/shard_map/dot_general | solution.py:64
  11.9 0.2 fusion.50
  12.2 2.0 %fusion.14 = f32[16,512]{1,0:T(8,128)S(1)} fusion(bf16[2048,512]{1,0:T(8,128)(2,1)} %param.23, bf16[16,2048]{1,0:T(8,128)(2,1)S(1)} %copy-done.3, f32[2048]{0:T(1024)S(1)} %copy-done.5, f32[16]{0:T(128)S(1)} %add_rsqrt_fusion.4), kind=kOutput, calls=%fused_computation.15 | convolution fusion | flops 33701888 | bytes 2203712 | tf_op jit(solution)/shard_map/dot_general | solution.py:65
  14.2 2.0 %fusion.16 = f32[16,512]{1,0:T(8,128)S(1)} fusion(bf16[2048,512]{1,0:T(8,128)(2,1)} %param.21, bf16[16,2048]{1,0:T(8,128)(2,1)S(1)} %copy-done.3, f32[2048]{0:T(1024)S(1)} %copy-done.5, f32[16]{0:T(128)S(1)} %add_rsqrt_fusion.4), kind=kOutput, calls=%fused_computation.19 | convolution fusion | flops 33701888 | bytes 2203712 | tf_op jit(solution)/shard_map/dot_general | solution.py:63
  16.6 5.5 %fusion.63 = f32[16,4,1,128]{3,2,1,0:T(1,128)S(1)} fusion(f32[16,4,128,1]{2,3,1,0:T(1,128)S(1)} %bitcast.68, f32[16,4,128,128]{3,2,1,0:T(8,128)} %param.19), kind=kOutput, calls=%fused_computation.91 | convolution fusion | flops 12582912 | bytes 4259840 | tf_op jit(solution)/shard_map/thd,thde->the/dot_general | solution.py:82
  22.2 1.5 %multiply_add_fusion = f32[16,4,128,128]{3,2,1,0:T(8,128)S(1)} fusion(f32[16,4,128,128]{3,2,1,0:T(8,128)S(1)} %copy-done.1, f32[16,4,128]{2,1,0:T(4,128)S(1)} %fusion.30, f32[16,4,128]{2,1,0:T(4,128)S(1)} %get-tuple-element.4, f32[16,4]{1,0:T(8,128)S(1)} %copy.39), kind=kLoop, calls=%fused_computation | loop fusion | flops 3145728 | bytes 8454400 | tf_op jit(solution)/shard_map/add | solution.py:86
  23.7 3.7 %fusion.64 = f32[16,4,1,128]{3,2,1,0:T(1,128)S(1)} fusion(f32[16,4,128,1]{2,3,1,0:T(1,128)S(1)} %bitcast.69, f32[16,4,128,128]{3,2,1,0:T(8,128)S(1)} %multiply_add_fusion), kind=kOutput, calls=%fused_computation.92 | convolution fusion | flops 12582912 | bytes 4259840 | tf_op jit(solution)/shard_map/thd,thde->the/dot_general | solution.py:87
  27.5 0.4 fusion.13
  28.1 2.0 %fusion.33 = f32[16,2048]{1,0:T(8,128)S(1)} fusion(bf16[512,2048]{1,0:T(8,128)(2,1)} %param.29, bf16[2,8,4,128]{3,2,1,0:T(4,128)(2,1)S(1)} %bitcast.71), kind=kOutput, calls=%fused_computation.50 | convolution fusion | flops 33554432 | bytes 2244608 | tf_op jit(solution)/shard_map/dot_general | solution.py:93
  30.1 7.1 %all-gather = f32[32,2048]{1,0:T(8,128)S(1)} all-gather(f32[16,2048]{1,0:T(8,128)S(1)} %fusion.33), channel_id=2, replica_groups=mesh['ep'=16,'tp'=2] {'tp'}, dimensions={0}, use_global_device_ids=true | all-gather | bytes 393216 | tf_op jit(solution)/shard_map/all_gather | solution.py:11
  37.7 0.2 select_reduce_fusion
  38.1 0.3 convolution_convert_fusion
  38.5 30.8 %all_to_all.10 = bf16[16,16,2048]{2,1,0:T(8,128)(2,1)S(1)} all-to-all(bf16[16,16,2048]{2,1,0:T(8,128)(2,1)S(1)} %bitcast.59), channel_id=1, replica_groups=mesh['ep'=16,'tp'=2] {'ep'}, dimensions={0} | all-to-all | bytes 2097152 | tf_op jit(solution)/shard_map/all_to_all | solution.py:110
  69.4 0.7 fusion.4
  70.1 0.9 copy-done.11
  71.0 0.7 fusion.9
  71.7 2.1 %fusion = f32[16,16,2048]{2,1,0:T(8,128)} fusion(bf16[16,16,512]{2,1,0:T(8,128)(2,1)S(1)} %bitcast.67, bf16[1,512,2048]{2,1,0:T(8,128)(2,1)S(1)} %copy-done), kind=kOutput, calls=%fused_computation.2 | convolution fusion | flops 536870912 | bytes 4456448 | tf_op jit(solution)/shard_map/dot_general | solution.py:120
  73.8 32.4 %reduce-scatter.2.cloned.1.call-done = f32[16,16,1024]{2,1,0:T(8,128)} async-done(((f32[16,16,2048]{2,1,0:T(8,128)}), f32[16,16,1024]{2,1,0:T(8,128)}) %reduce-scatter.2.cloned.1.call-update) | async-done | bytes 1048592 | tf_op jit(solution)/shard_map/reduce_scatter | solution.py:123
  106.2 2.1 %convert_element_type.83 = bf16[16,16,1024]{2,1,0:T(8,128)(2,1)} convert(f32[16,16,1024]{2,1,0:T(8,128)} %reduce-scatter.2.cloned.1.call-done) | non-fusion elementwise | flops 262144 | bytes 1572864 | tf_op jit(solution)/shard_map/convert_element_type | solution.py:123
  108.3 5.6 %all-to-all-start.1 = ((bf16[16,16,1024]{2,1,0:T(8,128)(2,1)}), bf16[16,16,1024]{2,1,0:T(8,128)(2,1)S(1)}, u32[]{:S(2)}, u32[]{:S(2)}) async-start(bf16[16,16,1024]{2,1,0:T(8,128)(2,1)} %convert_element_type.83), calls=%async_computation.2 | async-start | bytes 1048576 | tf_op jit(solution)/shard_map/all_to_all | solution.py:124
  113.9 14.2 %all-to-all-done.1 = bf16[16,16,1024]{2,1,0:T(8,128)(2,1)S(1)} async-done(((bf16[16,16,1024]{2,1,0:T(8,128)(2,1)}), bf16[16,16,1024]{2,1,0:T(8,128)(2,1)S(1)}, u32[]{:S(2)}, u32[]{:S(2)}) %all-to-all-start.1) | async-done | bytes 524320 | tf_op jit(solution)/shard_map/all_to_all | solution.py:124
  128.3 0.9 fusion.12
  (63 shorter events, 2.2 us)
Async XLA Ops:
  7.2 64.5 %copy-start = (bf16[1,512,2048]{2,1,0:T(8,128)(2,1)S(1)}, bf16[1,512,2048]{2,1,0:T(8,128)(2,1)}, u32[]{:S(2)}) copy-start(bf16[1,512,2048]{2,1,0:T(8,128)(2,1)} %param.35) | copy-start | bytes 6291460
  7.2 4.7 %copy-start.3 = (bf16[16,2048]{1,0:T(8,128)(2,1)S(1)}, bf16[16,2048]{1,0:T(8,128)(2,1)}, u32[]{:S(2)}) copy-start(bf16[16,2048]{1,0:T(8,128)(2,1)} %param.18) | copy-start | bytes 196612
  7.2 4.7 %copy-start.5 = (f32[2048]{0:T(1024)S(1)}, f32[2048]{0:T(1024)}, u32[]{:S(2)}) copy-start(f32[2048]{0:T(1024)} %param.20) | copy-start | bytes 24580
  7.2 4.6 %copy-start.13 = (f32[8]{0:T(128)S(1)}, f32[8]{0:T(128)}, u32[]{:S(2)}) copy-start(f32[8]{0:T(128)} %param.27) | copy-start | bytes 100
  7.2 4.7 %copy-start.12 = (bf16[2048,8]{0,1:T(8,128)(2,1)S(1)}, bf16[2048,8]{0,1:T(8,128)(2,1)}, u32[]{:S(2)}) copy-start(bf16[2048,8]{0,1:T(8,128)(2,1)} %param.26) | copy-start | bytes 98308
  7.2 99.0 %reduce-scatter.2.cloned.1.call-start = ((), (), s32[]{:S(2)}) async-start(), calls=%async_computation.3 | async-start | bytes 3145728 | tf_op jit(solution)/shard_map/reduce_scatter | solution.py:123
  16.6 5.6 %copy-start.1 = (f32[16,4,128,128]{3,2,1,0:T(8,128)S(1)}, f32[16,4,128,128]{3,2,1,0:T(8,128)}, u32[]{:S(2)}) copy-start(f32[16,4,128,128]{3,2,1,0:T(8,128)} %param.19) | copy-start | bytes 12582916
  23.7 3.7 %copy-start.2 = (f32[16,4,128,128]{3,2,1,0:T(8,128)}, f32[16,4,128,128]{3,2,1,0:T(8,128)S(1)}, u32[]{:S(2)}) copy-start(f32[16,4,128,128]{3,2,1,0:T(8,128)S(1)} %multiply_add_fusion) | copy-start | bytes 12582916
  23.7 3.8 %copy-start.4 = (bf16[2048,512]{1,0:T(8,128)(2,1)S(1)}, bf16[2048,512]{1,0:T(8,128)(2,1)}, u32[]{:S(2)}) copy-start(bf16[2048,512]{1,0:T(8,128)(2,1)} %param.24) | copy-start | bytes 6291460
  27.4 0.7 copy-start.9
  27.9 9.5 %copy-start.7 = (s32[16,2]{0,1:T(2,128)S(1)}, s32[16,2]{0,1:T(2,128)}, u32[]{:S(2)}) copy-start(s32[16,2]{0,1:T(2,128)} %param.31) | copy-start | bytes 388
  27.9 10.2 %copy-start.6 = (f32[2048]{0:T(1024)S(1)}, f32[2048]{0:T(1024)}, u32[]{:S(2)}) copy-start(f32[2048]{0:T(1024)} %param.30) | copy-start | bytes 24580
  38.0 31.3 %copy-start.10 = (bf16[1,2048,512]{2,1,0:T(8,128)(2,1)S(1)}, bf16[1,2048,512]{2,1,0:T(8,128)(2,1)}, u32[]{:S(2)}) copy-start(bf16[1,2048,512]{2,1,0:T(8,128)(2,1)} %param.33) | copy-start | bytes 6291460
  69.4 1.6 %copy-start.11 = (bf16[1,2048,512]{2,1,0:T(8,128)(2,1)S(1)}, bf16[1,2048,512]{2,1,0:T(8,128)(2,1)}, u32[]{:S(2)}) copy-start(bf16[1,2048,512]{2,1,0:T(8,128)(2,1)} %param.34) | copy-start | bytes 6291460
  73.8 40.2 %copy-start.8 = (f32[16,2]{0,1:T(2,128)S(1)}, f32[16,2]{0,1:T(2,128)}, u32[]{:S(2)}) copy-start(f32[16,2]{0,1:T(2,128)} %param.32) | copy-start | bytes 388
  108.3 19.9 %all-to-all-start.1 = ((bf16[16,16,1024]{2,1,0:T(8,128)(2,1)}), bf16[16,16,1024]{2,1,0:T(8,128)(2,1)S(1)}, u32[]{:S(2)}, u32[]{:S(2)}) async-start(bf16[16,16,1024]{2,1,0:T(8,128)(2,1)} %convert_element_type.83), calls=%async_computation.2 | async-start | bytes 1048576 | tf_op jit(solution)/shard_map/all_to_all | solution.py:124
Sparse Core Ops, SparseCore 0:
  73.9 32.2 reduce-scatter.1
